TPU v7x, 32 devices: a whole 2x2x4 slice. The times are simulated.
32 devices in a mesh: sp: 16 (over z, x, core), tp: 2 (over y).
Axes of the slice: x: 2, y: 2, z: 4, core: 2. Of those that a mesh axis runs over, the one named last changes fastest.
Arguments:
- residual: bfloat16 [4096, 2048], P(('sp', 'tp')), may hold values from -6 to 6
- query_vectors: bfloat16 [4096, 512], P('sp', 'tp'), may hold values from -6 to 6
- key_vectors: bfloat16 [4096, 512], P('sp', 'tp'), may hold values from -6 to 6
- value_vectors: bfloat16 [4096, 512], P('sp', 'tp'), may hold values from -6 to 6
- in_gate: float32 [8, 4096], P('tp', 'sp'), may hold values from -9 to 190
- forget_gate: float32 [8, 4096], P('tp', 'sp'), may hold values from -1 to 12
- documents: int32 [4096], P('sp'), may hold values from 0 to 3, never falling along the last dimension, each value on 1 to 2048 neighbouring positions
- w_out: bfloat16 [512, 2048], P('tp'), may hold values from -0.25 to 0.25
- norm_gain: bfloat16 [2048], replicated, may hold values from 0.099609375 to 1.8984375
- w_up: bfloat16 [2048, 8192], P('sp', 'tp'), may hold values from -0.125 to 0.125
- w_down: bfloat16 [8192, 2048], P('tp', 'sp'), may hold values from -0.0625 to 0.0625
Outputs:
- layer_out: bfloat16 [4096, 2048], P(('sp', 'tp'))
Inputs may be any that keep to these rules, and one draw needn't show every extreme that they name: `documents`: document numbers never fall along the positions; every document has 1 to 2048 positions.
All inputs are finite; a program needn't handle non-finite values.
Results may differ from a plain program's by a relative error of at most 0.015.
Values may be sent and summed in bfloat16 or wider, within the bound.
A program may use at most 128 MiB of HBM per device.

v0:
```python
import jax
import jax.numpy as jnp
from jax import lax
from jax.sharding import PartitionSpec as P

SPAN = 128
very_negative = -1e30
epsilon = 1e-06


def carried_in(value, axis, combine, identity):
    length, here = (lax.axis_size(axis), lax.axis_index(axis))
    everything = jax.tree.map(lambda part: lax.all_gather(part, axis), value)
    start = jax.tree.map(
        lambda part, zero: jnp.broadcast_to(jnp.asarray(zero, part.dtype), part.shape),
        value,
        identity,
    )

    def lap(k, before):
        reached = k < here
        new = combine(before, jax.tree.map(lambda part: part[k], everything))
        return jax.tree.map(lambda a, b: jnp.where(reached, a, b), new, before)

    return lax.fori_loop(0, length, lap, start)


def identity_state(head_count, head_dim):
    return (
        jnp.zeros((head_count, head_dim, head_dim), jnp.float32),
        jnp.zeros((head_count, head_dim), jnp.float32),
        jnp.full((head_count,), very_negative, jnp.float32),
        jnp.zeros((head_count,), jnp.float32),
        jnp.array(-1.0, jnp.float32),
        jnp.array(-1.0, jnp.float32),
    )


def combine(earlier, later):
    memory_one, normal_one, top_one, decay_one, first_one, last_one = earlier
    memory_two, normal_two, top_two, decay_two, first_two, last_two = later
    later_empty = first_two < 0.0
    earlier_empty = first_one < 0.0
    keep = later_empty | (first_two == last_two) & (first_two == last_one)
    decay_step = jnp.where(later_empty, 0.0, decay_two)
    top_new = jnp.where(keep, jnp.maximum(decay_step + top_one, top_two), top_two)
    scale_old = jnp.where(keep, jnp.exp(decay_step + top_one - top_new), 0.0)
    scale_new = jnp.exp(top_two - top_new)
    memory_new = scale_old[:, None, None] * memory_one + scale_new[:, None, None] * memory_two
    normal_new = scale_old[:, None] * normal_one + scale_new[:, None] * normal_two
    decay_new = jnp.where(keep, decay_one + decay_step, decay_two)
    first_new = jnp.where(earlier_empty, first_two, first_one)
    last_new = jnp.where(later_empty, last_one, last_two)
    return (memory_new, normal_new, top_new, decay_new, first_new, last_new)


def block_summary(key_block, value_block, gate_block, decay_block, segment):
    cumulative = jnp.cumsum(decay_block, axis=-1)
    latest = segment == segment[-1]
    growth = jnp.where(latest[None, :], cumulative[:, -1:] - cumulative + gate_block, very_negative)
    top_log = jnp.max(growth, axis=-1)
    weight_table = jnp.exp(growth - top_log[:, None])
    key_expanded = key_block.astype(jnp.float32)
    value_expanded = value_block.astype(jnp.float32)
    memory_matrix = jnp.einsum(
        "jw,wjm,wju->jmu",
        weight_table,
        key_expanded,
        value_expanded,
        precision=lax.Precision.HIGHEST,
    )
    normal = jnp.einsum("hs,shk->hk", weight_table, key_expanded, precision=lax.Precision.HIGHEST)
    return (memory_matrix, normal, top_log, cumulative[:, -1], segment[0], segment[-1])


def block_output(query_block, key_block, value_block, gate_block, decay_block, segment, state):
    memory_matrix, normal, top_log, total_decay, first_doc, last_doc = state
    head_dim = query_block.shape[2]
    length = segment.shape[0]
    cumulative = jnp.cumsum(decay_block, axis=-1)
    row_ids = lax.broadcasted_iota(jnp.int32, (length, length), 0)
    col_ids = lax.broadcasted_iota(jnp.int32, (length, length), 1)
    allowed = (col_ids <= row_ids) & (segment[:, None] == segment[None, :])
    inside = jnp.where(
        allowed[None],
        cumulative[:, :, None] - cumulative[:, None, :] + gate_block[:, None, :],
        very_negative,
    )
    outside = jnp.where(
        (segment == last_doc)[None, :], cumulative + top_log[:, None], very_negative
    )
    peak_log = jnp.maximum(outside, jnp.max(inside, axis=-1))
    carried = jnp.exp(outside - peak_log)
    scaled = query_block * jnp.asarray(head_dim ** (-0.5), query_block.dtype)
    scores = jnp.einsum("lhd,shd->hls", scaled, key_block, preferred_element_type=jnp.float32)
    weight_table = jnp.exp(inside - peak_log[:, :, None]) * scores
    from_block = jnp.einsum(
        "hls,shv->hlv",
        weight_table.astype(jnp.bfloat16),
        value_block,
        preferred_element_type=jnp.float32,
    )
    scaled_expanded = scaled.astype(jnp.float32)
    memory_readout = jnp.einsum(
        "pug,uga->upa", scaled_expanded, memory_matrix, precision=lax.Precision.HIGHEST
    )
    numer_part = carried[:, :, None] * memory_readout + from_block
    denom_part = carried * jnp.einsum(
        "lhk,hk->hl", scaled_expanded, normal, precision=lax.Precision.HIGHEST
    ) + jnp.sum(weight_table, axis=-1)
    result = numer_part / jnp.maximum(jnp.abs(denom_part), jnp.exp(-peak_log))[:, :, None]
    return jnp.transpose(result, (1, 0, 2)).reshape(length, -1).astype(jnp.bfloat16)


def on_device(
    residual,
    query_vectors,
    key_vectors,
    value_vectors,
    in_gate,
    forget_gate,
    documents,
    w_out,
    norm_gain,
    w_up,
    w_down,
):
    tok_rows = query_vectors.shape[0]
    local_heads = in_gate.shape[0]
    head_dim = query_vectors.shape[1] // local_heads
    block_count = tok_rows // SPAN

    def to_blocks(vectors):
        return vectors.reshape(block_count, SPAN, local_heads, head_dim)

    def gate_blocks(gates):
        return jnp.transpose(gates.reshape(local_heads, block_count, SPAN), (1, 0, 2))

    query_blocks = to_blocks(query_vectors)
    key_blocks = to_blocks(key_vectors)
    value_blocks = to_blocks(value_vectors)
    input_blocks = gate_blocks(in_gate)
    decay_blocks = gate_blocks(jax.nn.log_sigmoid(forget_gate))
    segments = documents.astype(jnp.float32).reshape(block_count, SPAN)
    summaries = jax.vmap(block_summary)(
        key_blocks, value_blocks, input_blocks, decay_blocks, segments
    )
    empty_state = identity_state(local_heads, head_dim)

    def prefix_step(state, summary):
        return (combine(state, summary), state)

    device_total, prefixes = lax.scan(prefix_step, empty_state, summaries)
    incoming = carried_in(device_total, "sp", combine, empty_state)
    entering = jax.vmap(combine, in_axes=(None, 0))(incoming, prefixes)
    mixed = jax.vmap(block_output)(
        query_blocks, key_blocks, value_blocks, input_blocks, decay_blocks, segments, entering
    )
    mixed = mixed.reshape(tok_rows, local_heads * head_dim)
    regrouped = lax.all_to_all(mixed, "tp", split_axis=0, concat_axis=1, tiled=True)
    columns = regrouped
    projected = jnp.dot(
        columns, lax.all_gather(w_out, "tp", axis=0, tiled=True), preferred_element_type=jnp.float32
    )
    middle = (residual.astype(jnp.float32) + projected).astype(jnp.bfloat16)
    middle_wide = middle.astype(jnp.float32)
    factor = lax.rsqrt(jnp.mean(middle_wide * middle_wide, axis=-1, keepdims=True) + epsilon)
    normed = (middle_wide * factor * norm_gain.astype(jnp.float32)).astype(jnp.bfloat16)
    gathered = lax.all_gather(normed, "tp", axis=0, tiled=True)
    columns = gathered
    lifted = jnp.dot(
        columns, lax.all_gather(w_up, "sp", axis=0, tiled=True), preferred_element_type=jnp.float32
    )
    hidden = jnp.square(jax.nn.relu(lifted)).astype(jnp.bfloat16)
    terms = jnp.dot(
        hidden, lax.all_gather(w_down, "sp", axis=1, tiled=True), preferred_element_type=jnp.float32
    )
    summed = lax.psum_scatter(
        terms.astype(jnp.bfloat16), "tp", scatter_dimension=0, tiled=True
    ).astype(jnp.float32)
    return (middle_wide + summed).astype(jnp.bfloat16)


def solution(mesh):
    placed = (
        P(("sp", "tp"), None),
        P("sp", "tp"),
        P("sp", "tp"),
        P("sp", "tp"),
        P("tp", "sp"),
        P("tp", "sp"),
        P("sp"),
        P("tp", None),
        P(),
        P("sp", "tp"),
        P("tp", "sp"),
    )
    return jax.shard_map(
        on_device, mesh=mesh, in_specs=placed, out_specs=P(("sp", "tp"), None), check_vma=False
    )
```

profile of v0, /device:TPU:0, one launch (start us, length us, event | category | flops | bytes accessed | tf_op | source)
XLA Modules:
  0.0 511.1 jit_solution(8846787200100752153)
XLA Ops:
  6.5 0.7 fusion.36
  7.3 0.6 reduce_window_sum.12
  8.1 0.7 convert_bitcast_fusion
  8.9 0.8 broadcast_compare_fusion.1
  9.7 0.8 fusion.42
  10.5 0.8 fusion.59
  11.3 0.8 subtract_exponential_fusion.2
  12.2 1.0 copy.53
  13.2 1.1 reshape.152
  15.3 11.2 %while.55 = (s32[]{:T(128)}, f32[4,64,64]{2,1,0:T(8,128)S(1)}, f32[4,64]{1,0:T(4,128)S(1)}, f32[4]{0:T(128)S(1)}, f32[4]{0:T(128)S(1)}, /*index=5*/f32[]{:T(128)...) while((s32[]{:T(128)}, f32[4,64,64]{2,1,0:T(8,128)S(1)}, ...), condition=%wide.region_3.4_spmd.clone.clone, body=%wide.region_2.3_spmd.clone.sunk.clone | while | flops 83255 | bytes 466630 | solution.py:153
  15.3 0.6 dynamic_slice.131
  15.9 0.6 dynamic_slice.132
  20.9 0.6 dynamic_slice.131
  21.5 0.6 dynamic_slice.132
  26.5 0.7 copy-done
  27.2 0.7 all-gather.11.cloned.1.call-update
  29.6 0.7 dynamic-update-slice
  30.2 0.7 dynamic-update-slice.1
  30.9 35.2 %all-reduce.4 = (f32[16]{0:T(128)S(1)}, f32[16]{0:T(128)S(1)}, f32[64]{0:T(128)S(1)}, f32[64]{0:T(128)S(1)}) all-reduce(f32[16]{0:T(128)S(1)} %dynamic-update-slice, f32[16]{0:T(128)S(1)} %dynamic-update-slice.1, f32[64]{0:T(128)S(1)} %dynamic-update-slice.2, f32[64]{0:T(128)S(1)} %dynamic-update-slice.3), channel_id=1, replica_groups=mesh['sp'=16,'tp'=2] {'sp'}, use_global_device_ids=true, to_apply=%add | all-reduce | flops 160 | bytes 1280
  66.3 17.2 %all-gather.4 = f32[16,4,64]{2,1,0:T(4,128)S(1)} all-gather(f32[1,4,64]{2,1,0:T(4,128)S(1)} %bitcast.198), channel_id=5, replica_groups=mesh['sp'=16,'tp'=2] {'sp'}, dimensions={0}, use_global_device_ids=true | all-gather | bytes 17408 | tf_op jit(solution)/shard_map/all_gather | solution.py:13
  84.4 91.4 %while.56 = (s32[]{:T(128)}, f32[4,64,64]{2,1,0:T(8,128)S(1)}, f32[4,64]{1,0:T(4,128)S(1)}, f32[4]{0:T(128)S(1)}, f32[]{:T(128)}, /*index=5*/s32[]{:T(128)}, f32...) while((s32[]{:T(128)}, f32[4,64,64]{2,1,0:T(8,128)S(1)}, ...), condition=%wide.region_5.6_spmd.clone.clone, body=%wide.region_4.5_spmd.clone.sunk.clone | while | flops 83247 | bytes 200163 | solution.py:25
  85.0 0.6 dynamic_slice.136
  88.3 1.0 fusion.70
  90.7 0.6 dynamic_slice.136
  94.0 1.0 fusion.70
  96.4 0.6 dynamic_slice.136
  99.7 1.0 fusion.70
  102.1 0.6 dynamic_slice.136
  105.4 1.0 fusion.70
  107.8 0.6 dynamic_slice.136
  111.2 1.0 fusion.70
  113.5 0.6 dynamic_slice.136
  116.9 1.0 fusion.70
  119.2 0.6 dynamic_slice.136
  122.6 1.0 fusion.70
  125.0 0.6 dynamic_slice.136
  128.3 1.0 fusion.70
  130.7 0.6 dynamic_slice.136
  134.0 1.0 fusion.70
  136.4 0.6 dynamic_slice.136
  139.7 1.0 fusion.70
  142.1 0.6 dynamic_slice.136
  145.4 1.0 fusion.70
  147.8 0.6 dynamic_slice.136
  151.1 1.0 fusion.70
  153.5 0.6 dynamic_slice.136
  156.8 1.0 fusion.70
  159.2 0.6 dynamic_slice.136
  162.6 1.0 fusion.70
  164.9 0.6 dynamic_slice.136
  168.3 1.0 fusion.70
  170.6 0.6 dynamic_slice.136
  174.0 1.0 fusion.70
  177.4 0.9 fusion.21
  178.2 3.4 all-to-all-start
  181.7 4.5 all-to-all-done
  186.2 2.1 multiply_reduce_fusion
  188.3 1.0 multiply_convert_fusion
  190.5 18.0 %all-gather.13.cloned.1.call-done = bf16[256,2048]{1,0:T(8,128)(2,1)} async-done(((bf16[128,2048]{1,0:T(8,128)(2,1)}), bf16[256,2048]{1,0:T(8,128)(2,1)}) %all-gather.13.cloned.1.call-update) | async-done | bytes 1048592 | tf_op jit(solution)/shard_map/all_gather | solution.py:169
  208.5 128.5 %all-gather.15.cloned.1.call-done = bf16[2048,4096]{1,0:T(8,128)(2,1)} async-done(((bf16[128,4096]{1,0:T(8,128)(2,1)}), bf16[2048,4096]{1,0:T(8,128)(2,1)}) %all-gather.15.cloned.1.call-update) | async-done | bytes 16777232 | tf_op jit(solution)/shard_map/all_gather | solution.py:172
  337.0 130.1 %all-gather.17.cloned.1.call-done = bf16[4096,2048]{1,0:T(8,128)(2,1)} async-done(((bf16[4096,128]{1,0:T(8,128)(2,1)}), bf16[4096,2048]{1,0:T(8,128)(2,1)}) %all-gather.17.cloned.1.call-update) | async-done | bytes 16777232 | tf_op jit(solution)/shard_map/all_gather | solution.py:176
  467.1 16.5 %convolution_convert_fusion = bf16[256,2048]{1,0:T(8,128)(2,1)} fusion(bf16[4096,2048]{1,0:T(8,128)(2,1)} %all-gather.17.cloned.1.call-done, bf16[256,2048]{1,0:T(8,128)(2,1)} %all-gather.13.cloned.1.call-done, bf16[2048,4096]{1,0:T(8,128)(2,1)} %all-gather.15.cloned.1.call-done), kind=kOutput, calls=%fused_computation.40 | convolution fusion | flops 8593604608 | bytes 35651584 | tf_op jit(solution)/shard_map/dot_general | solution.py:175
  483.6 18.7 %reduce-scatter.2.cloned.1.call-done = bf16[128,2048]{1,0:T(8,128)(2,1)} async-done(((bf16[256,2048]{1,0:T(8,128)(2,1)}), bf16[128,2048]{1,0:T(8,128)(2,1)}) %reduce-scatter.2.cloned.1.call-update) | async-done | bytes 524304 | tf_op jit(solution)/shard_map/reduce_scatter | solution.py:178
  502.3 2.0 add_convert_fusion
  (161 shorter events, 18.7 us)
Async XLA Ops:
  6.5 21.5 %copy-start.6 = (u32[32]{0:T(128)S(1)}, u32[32]{0:T(128)}, u32[]{:S(2)}) copy-start(u32[32]{0:T(128)} %constant.91) | copy-start | bytes 388
  6.5 77.0 %copy-start.2 = (bf16[256,256]{1,0:T(8,128)(2,1)S(1)}, bf16[256,256]{1,0:T(8,128)(2,1)}, u32[]{:S(2)}) copy-start(bf16[256,256]{1,0:T(8,128)(2,1)} %param.16) | copy-start | bytes 393220
  6.5 77.8 %all-gather.19.cloned.1.call-start = ((), (), s32[]{:S(2)}) async-start(), calls=%async_computation.7 | async-start | bytes 2228224 | tf_op jit(solution)/shard_map/all_gather | solution.py:13
  13.2 70.8 %copy-start.3 = (f32[4,256]{1,0:T(4,128)S(1)}, f32[4,256]{1,0:T(4,128)}, u32[]{:S(2)}) copy-start(f32[4,256]{1,0:T(4,128)} %param.19) | copy-start | bytes 12292
  15.2 160.6 %copy-start.4 = (s32[256]{0:T(256)S(1)}, s32[256]{0:T(256)}, u32[]{:S(2)}) copy-start(s32[256]{0:T(256)} %param.21) | copy-start | bytes 3076
  26.5 0.7 copy-start
  27.2 154.5 %copy-start.5 = (bf16[2048]{0:T(1024)(128)(2,1)S(1)}, bf16[2048]{0:T(1024)(128)(2,1)}, u32[]{:S(2)}) copy-start(bf16[2048]{0:T(1024)(128)(2,1)} %param.23) | copy-start | bytes 12292
  27.2 159.0 %copy-start.1 = (bf16[128,2048]{1,0:T(8,128)(2,1)S(1)}, bf16[128,2048]{1,0:T(8,128)(2,1)}, u32[]{:S(2)}) copy-start(bf16[128,2048]{1,0:T(8,128)(2,1)} %param.15) | copy-start | bytes 1572868
  27.2 159.0 %all-gather.11.cloned.1.call-start = ((), (), s32[]{:S(2)}) async-start(), calls=%async_computation.2 | async-start | bytes 3145728 | tf_op jit(solution)/shard_map/all_gather | solution.py:163
  178.2 7.9 %all-to-all-start = ((bf16[2,128,256]{1,2,0:T(8,128)(2,1)}), bf16[2,128,256]{1,2,0:T(8,128)(2,1)S(1)}, u32[]{:S(2)}, u32[]{:S(2)}) async-start(bf16[2,128,256]{1,2,0:T(8,128)(2,1)} %bitcast.27), calls=%async_computation | async-start | bytes 262144 | tf_op jit(solution)/shard_map/all_to_all | solution.py:160
  181.6 26.9 %all-gather.13.cloned.1.call-start = ((), (), s32[]{:S(2)}) async-start(), calls=%async_computation.3 | async-start | bytes 1572864 | tf_op jit(solution)/shard_map/all_gather | solution.py:169
  189.3 147.7 %all-gather.15.cloned.1.call-start = ((), (), s32[]{:S(2)}) async-start(), calls=%async_computation.4 | async-start | bytes 17825792 | tf_op jit(solution)/shard_map/all_gather | solution.py:172
  189.9 277.2 %all-gather.17.cloned.1.call-start = ((), (), s32[]{:S(2)}) async-start(), calls=%async_computation.5 | async-start | bytes 17825792 | tf_op jit(solution)/shard_map/all_gather | solution.py:176
  190.5 311.8 %reduce-scatter.2.cloned.1.call-start = ((), (), s32[]{:S(2)}) async-start(), calls=%async_computation.6 | async-start | bytes 1572864 | tf_op jit(solution)/shard_map/reduce_scatter | solution.py:178
Sparse Core Ops, SparseCore 0:
  27.3 44.1 all-gather.18
  73.0 31.7 all-gather.10
  189.4 19.0 all-gather.12
  210.5 126.4 all-gather.14
  339.0 128.0 all-gather.16
  483.7 18.5 reduce-scatter.1
where the time goes:
time: 513 us; the launch traced here: 511 us
  waiting for transfers between devices  302 us (59%)
  loops' own time  61.4 us (12%)
  blocking collectives  52.5 us (10%)
  local copies, waits for them, and re-layouts  28.9 us (6%)
  other arithmetic  27.6 us (5%)
  matrix products  21.3 us (4%)
  between operations  14.4 us (3%)
    all_gather x1, waiting for transfers between devices, on_device(): lax.all_gather(w_down, 'sp', axis=1, tiled=True)  130 us
    all_gather x1, waiting for transfers between devices, on_device(): lax.all_gather(w_up, 'sp', axis=0, tiled=True)  128 us
    another operation x1, loops' own time, carried_in(): return lax.fori_loop(0, length, lap, start)  53.6 us
    unnamed x1, blocking collectives  35.2 us
    dynamic_slice x32, local copies, waits for them, and re-layouts, lap(): new = combine(before, jax.tree.map(lambda part: part[k], everything))  19.7 us
    reduce_scatter x1, waiting for transfers between devices, on_device(): lax.psum_scatter(terms.astype(jnp.bfloat16), 'tp', scatter_dimension=0, t...  18.7 us
    all_gather x1, waiting for transfers between devices, on_device(): gathered = lax.all_gather(normed, 'tp', axis=0, tiled=True)  18 us
    select_n x48, other arithmetic, lap(): return jax.tree.map(lambda a, b: jnp.where(reached, a, b), new, before)  17.7 us
  transfers between devices with their start and end apart: 7, of which 5 were waited for; matrix products, arithmetic and copies ran while one was open for 9% of the time, Pallas kernels for 0%

commit v1 on v0

--- a/solution.py
+++ b/solution.py
@@ -173,7 +173,9 @@
     )
     hidden = jnp.square(jax.nn.relu(lifted)).astype(jnp.bfloat16)
     terms = jnp.dot(
-        hidden, lax.all_gather(w_down, "sp", axis=1, tiled=True), preferred_element_type=jnp.float32
+        hidden,
+        jnp.concatenate(lax.all_gather(w_down, "sp"), axis=1),
+        preferred_element_type=jnp.float32,
     )
     summed = lax.psum_scatter(
         terms.astype(jnp.bfloat16), "tp", scatter_dimension=0, tiled=True

time: 513 us -> 429 us (0.84)
  waiting for transfers between devices: 302 us -> 202 us
  local copies, waits for them, and re-layouts: 28.9 us -> 49 us
    all_gather x1, waiting for transfers between devices: 130 us -> 48.2 us  [on_device(): lax.all_gather(w_down, 'sp')]
    reshape x0 -> x1, local copies, waits for them, and re-layouts: none -> 21.3 us  [on_device(): jnp.concatenate(lax.all_gather(w_down, 'sp'), axis=1)]
    all_gather x1, waiting for transfers between devices: 18 us -> 0.01 us  [on_device(): gathered = lax.all_gather(normed, 'tp', axis=0, tiled=True)]
  transfers between devices with their start and end apart: 7 -> 7, of which waited for: 5 -> 4; matrix products, arithmetic and copies ran while one was open for 9% -> 16% of each run, Pallas kernels for 0% -> 0%
where the time goes in v1:
time: 429 us; the launch traced here: 427 us
  waiting for transfers between devices  202 us (47%)
  loops' own time  57.1 us (13%)
  blocking collectives  52.4 us (12%)
  local copies, waits for them, and re-layouts  49 us (11%)
  other arithmetic  27.6 us (6%)
  matrix products  21.3 us (5%)
  between operations  14.5 us (3%)
    all_gather x1, waiting for transfers between devices, on_device(): lax.all_gather(w_up, 'sp', axis=0, tiled=True)  128 us
    another operation x1, loops' own time, carried_in(): return lax.fori_loop(0, length, lap, start)  49.4 us
    all_gather x1, waiting for transfers between devices, on_device(): lax.all_gather(w_down, 'sp')  48.2 us
    unnamed x1, blocking collectives  35.2 us
    reshape x1, local copies, waits for them, and re-layouts, on_device(): jnp.concatenate(lax.all_gather(w_down, 'sp'), axis=1)  21.3 us
    reduce_scatter x1, waiting for transfers between devices, on_device(): lax.psum_scatter(terms.astype(jnp.bfloat16), 'tp', scatter_dimension=0, t...  18.7 us
    dynamic_slice x32, local copies, waits for them, and re-layouts, lap(): new = combine(before, jax.tree.map(lambda part: part[k], everything))  18.2 us
    select_n x48, other arithmetic, lap(): return jax.tree.map(lambda a, b: jnp.where(reached, a, b), new, before)  17.8 us
  transfers between devices with their start and end apart: 7, of which 4 were waited for; matrix products, arithmetic and copies ran while one was open for 16% of the time, Pallas kernels for 0%

profile of v1, /device:TPU:0, one launch (start us, length us, event | category | flops | bytes accessed | tf_op | source)
XLA Modules:
  0.0 427.0 jit_solution(16880081216858877177)
XLA Ops:
  6.5 0.7 fusion.36
  7.2 0.6 reduce_window_sum.12
  8.0 0.7 convert_bitcast_fusion
  8.9 0.8 broadcast_compare_fusion.1
  9.7 0.8 fusion.42
  10.5 0.8 fusion.59
  11.3 0.8 subtract_exponential_fusion.2
  12.1 1.0 copy.54
  13.2 1.1 reshape.161
  15.3 11.2 %while.55 = (s32[]{:T(128)}, f32[4,64,64]{2,1,0:T(8,128)S(1)}, f32[4,64]{1,0:T(4,128)S(1)}, f32[4]{0:T(128)S(1)}, f32[4]{0:T(128)S(1)}, /*index=5*/f32[]{:T(128)...) while((s32[]{:T(128)}, f32[4,64,64]{2,1,0:T(8,128)S(1)}, ...), condition=%wide.region_3.4_spmd.clone.clone, body=%wide.region_2.3_spmd.clone.sunk.clone | while | flops 83255 | bytes 466630 | solution.py:153
  15.3 0.6 dynamic_slice.131
  15.9 0.6 dynamic_slice.132
  20.9 0.6 dynamic_slice.131
  21.5 0.6 dynamic_slice.132
  26.5 0.7 copy-done
  27.2 0.7 all-gather.12.cloned.1.call-update
  28.0 0.7 all-gather.20.cloned.1.call-update
  28.7 0.6 dynamic-slice
  30.5 0.8 dynamic-update-slice
  31.3 0.8 dynamic-update-slice.1
  32.1 35.2 %all-reduce.4 = (f32[16]{0:T(128)S(1)}, f32[16]{0:T(128)S(1)}, f32[64]{0:T(128)S(1)}, f32[64]{0:T(128)S(1)}) all-reduce(f32[16]{0:T(128)S(1)} %dynamic-update-slice, f32[16]{0:T(128)S(1)} %dynamic-update-slice.1, f32[64]{0:T(128)S(1)} %dynamic-update-slice.2, f32[64]{0:T(128)S(1)} %dynamic-update-slice.3), channel_id=1, replica_groups=mesh['sp'=16,'tp'=2] {'sp'}, use_global_device_ids=true, to_apply=%add | all-reduce | flops 160 | bytes 1280
  67.8 17.2 %all-gather.5 = f32[16,4,64]{2,1,0:T(4,128)S(1)} all-gather(f32[1,4,64]{2,1,0:T(4,128)S(1)} %bitcast.204), channel_id=5, replica_groups=mesh['sp'=16,'tp'=2] {'sp'}, dimensions={0}, use_global_device_ids=true | all-gather | bytes 17408 | tf_op jit(solution)/shard_map/all_gather | solution.py:13
  85.5 85.6 %while.56 = (s32[]{:T(128)}, f32[4,64,64]{2,1,0:T(8,128)S(1)}, f32[4,64]{1,0:T(4,128)S(1)}, f32[4]{0:T(128)S(1)}, f32[]{:T(128)}, /*index=5*/s32[]{:T(128)}, f32...) while((s32[]{:T(128)}, f32[4,64,64]{2,1,0:T(8,128)S(1)}, ...), condition=%wide.region_5.6_spmd.clone.clone, body=%wide.region_4.5_spmd.clone.sunk.clone | while | flops 83247 | bytes 200163 | solution.py:25
  85.5 0.6 dynamic_slice.135
  89.2 1.0 fusion.70
  90.8 0.6 dynamic_slice.135
  94.5 1.0 fusion.70
  96.2 0.6 dynamic_slice.135
  99.9 1.0 fusion.70
  101.5 0.6 dynamic_slice.135
  105.2 1.0 fusion.70
  106.9 0.6 dynamic_slice.135
  110.6 1.0 fusion.70
  112.2 0.6 dynamic_slice.135
  115.9 1.0 fusion.70
  117.6 0.6 dynamic_slice.135
  121.3 1.0 fusion.70
  122.9 0.6 dynamic_slice.135
  126.6 1.0 fusion.70
  128.3 0.6 dynamic_slice.135
  132.0 1.0 fusion.70
  133.6 0.6 dynamic_slice.135
  137.3 1.0 fusion.70
  142.6 1.0 fusion.70
  144.3 0.6 dynamic_slice.135
  148.0 1.0 fusion.70
  149.6 0.6 dynamic_slice.135
  153.3 1.0 fusion.70
  155.0 0.6 dynamic_slice.135
  158.7 1.1 fusion.70
  160.4 0.6 dynamic_slice.135
  164.1 1.0 fusion.70
  169.4 1.0 fusion.70
  172.7 0.9 fusion.21
  173.6 3.4 all-to-all-start
  177.0 4.5 %all-to-all-done = bf16[2,128,256]{1,2,0:T(8,128)(2,1)S(1)} async-done(((bf16[2,128,256]{1,2,0:T(8,128)(2,1)}), bf16[2,128,256]{1,2,0:T(8,128)(2,1)S(1)}, u32[]{:S(2)}, u32[]{:S(2)}) %all-to-all-start) | async-done | bytes 131104 | tf_op jit(solution)/shard_map/all_to_all | solution.py:160
  181.5 2.1 multiply_reduce_fusion
  183.7 1.0 multiply_convert_fusion
  185.3 48.2 %all-gather.20.cloned.1.call-done = bf16[65536,128]{1,0:T(8,128)(2,1)} async-done(((bf16[4096,128]{1,0:T(8,128)(2,1)}), bf16[65536,128]{1,0:T(8,128)(2,1)}) %all-gather.20.cloned.1.call-update) | async-done | bytes 16777232 | tf_op jit(solution)/shard_map/all_gather | solution.py:177
  233.5 21.3 %copy.65 = bf16[4096,16,128]{0,2,1:T(8,128)(2,1)} copy(bf16[4096,16,128]{2,0,1:T(8,128)(2,1)} %bitcast.201) | data formatting | bytes 33554432 | tf_op jit(solution)/shard_map/reshape | solution.py:177
  254.8 128.1 %all-gather.16.cloned.1.call-done = bf16[2048,4096]{1,0:T(8,128)(2,1)} async-done(((bf16[128,4096]{1,0:T(8,128)(2,1)}), bf16[2048,4096]{1,0:T(8,128)(2,1)}) %all-gather.16.cloned.1.call-update) | async-done | bytes 16777232 | tf_op jit(solution)/shard_map/all_gather | solution.py:172
  383.0 16.5 %convolution_convert_fusion = bf16[256,2048]{1,0:T(8,128)(2,1)} fusion(bf16[4096,2048]{0,1:T(8,128)(2,1)} %bitcast.202, bf16[256,2048]{1,0:T(8,128)(2,1)} %all-gather.14.cloned.1.call-done, bf16[2048,4096]{1,0:T(8,128)(2,1)} %all-gather.16.cloned.1.call-done), kind=kOutput, calls=%fused_computation.40 | convolution fusion | flops 8593604608 | bytes 35651584 | tf_op jit(solution)/shard_map/dot_general | solution.py:175
  399.4 18.7 %reduce-scatter.2.cloned.1.call-done = bf16[128,2048]{1,0:T(8,128)(2,1)} async-done(((bf16[256,2048]{1,0:T(8,128)(2,1)}), bf16[128,2048]{1,0:T(8,128)(2,1)}) %reduce-scatter.2.cloned.1.call-update) | async-done | bytes 524304 | tf_op jit(solution)/shard_map/reduce_scatter | solution.py:180
  418.2 2.0 add_convert_fusion
  (162 shorter events, 18.1 us)
Async XLA Ops:
  6.5 78.9 %all-gather.18.cloned.1.call-start = ((), (), s32[]{:S(2)}) async-start(), calls=%async_computation.6 | async-start | bytes 2228224 | tf_op jit(solution)/shard_map/all_gather | solution.py:13
  13.1 15.6 %copy-start.6 = (u32[32]{0:T(128)S(1)}, u32[32]{0:T(128)}, u32[]{:S(2)}) copy-start(u32[32]{0:T(128)} %constant.91) | copy-start | bytes 388
  13.1 54.3 %copy-start.2 = (bf16[256,256]{1,0:T(8,128)(2,1)S(1)}, bf16[256,256]{1,0:T(8,128)(2,1)}, u32[]{:S(2)}) copy-start(bf16[256,256]{1,0:T(8,128)(2,1)} %param.16) | copy-start | bytes 393220
  14.6 70.5 %copy-start.3 = (f32[4,256]{1,0:T(4,128)S(1)}, f32[4,256]{1,0:T(4,128)}, u32[]{:S(2)}) copy-start(f32[4,256]{1,0:T(4,128)} %param.19) | copy-start | bytes 12292
  15.2 155.9 %copy-start.4 = (s32[256]{0:T(256)S(1)}, s32[256]{0:T(256)}, u32[]{:S(2)}) copy-start(s32[256]{0:T(256)} %param.21) | copy-start | bytes 3076
  26.5 0.7 copy-start
  27.2 154.3 %all-gather.12.cloned.1.call-start = ((), (), s32[]{:S(2)}) async-start(), calls=%async_computation.2 | async-start | bytes 3145728 | tf_op jit(solution)/shard_map/all_gather | solution.py:163
  27.9 149.1 %copy-start.5 = (bf16[2048]{0:T(1024)(128)(2,1)S(1)}, bf16[2048]{0:T(1024)(128)(2,1)}, u32[]{:S(2)}) copy-start(bf16[2048]{0:T(1024)(128)(2,1)} %param.23) | copy-start | bytes 12292
  27.9 153.6 %copy-start.1 = (bf16[128,2048]{1,0:T(8,128)(2,1)S(1)}, bf16[128,2048]{1,0:T(8,128)(2,1)}, u32[]{:S(2)}) copy-start(bf16[128,2048]{1,0:T(8,128)(2,1)} %param.15) | copy-start | bytes 1572868
  28.0 205.6 %all-gather.20.cloned.1.call-start = ((), (), s32[]{:S(2)}) async-start(), calls=%async_computation.7 | async-start | bytes 17825792 | tf_op jit(solution)/shard_map/all_gather | solution.py:177
  173.6 7.9 %all-to-all-start = ((bf16[2,128,256]{1,2,0:T(8,128)(2,1)}), bf16[2,128,256]{1,2,0:T(8,128)(2,1)S(1)}, u32[]{:S(2)}, u32[]{:S(2)}) async-start(bf16[2,128,256]{1,2,0:T(8,128)(2,1)} %bitcast.27), calls=%async_computation | async-start | bytes 262144 | tf_op jit(solution)/shard_map/all_to_all | solution.py:160
  177.0 77.9 %all-gather.14.cloned.1.call-start = ((), (), s32[]{:S(2)}) async-start(), calls=%async_computation.3 | async-start | bytes 1572864 | tf_op jit(solution)/shard_map/all_gather | solution.py:169
  184.6 198.3 %all-gather.16.cloned.1.call-start = ((), (), s32[]{:S(2)}) async-start(), calls=%async_computation.4 | async-start | bytes 17825792 | tf_op jit(solution)/shard_map/all_gather | solution.py:172
  185.2 232.9 %reduce-scatter.2.cloned.1.call-start = ((), (), s32[]{:S(2)}) async-start(), calls=%async_computation.5 | async-start | bytes 1572864 | tf_op jit(solution)/shard_map/reduce_scatter | solution.py:180
Sparse Core Ops, SparseCore 0:
  27.3 44.2 all-gather.17
  73.1 31.8 all-gather.11
  107.1 126.3 all-gather.19
  234.9 19.5 all-gather.13
  256.5 126.4 all-gather.15
  399.6 18.5 reduce-scatter.1
